TPU v7x, 32 devices: a whole 2x2x4 slice. The times are simulated.
32 devices in a mesh: sp: 8 (over z, x), tp: 4 (over y, core).
Axes of the slice: x: 2, y: 2, z: 4, core: 2. Of those that a mesh axis runs over, the one named last changes fastest.
Arguments:
- tokens: bfloat16 [2048, 3072], P('sp', 'tp'), may hold values from -6 to 6
- norm_gain: float32 [3072], replicated, may hold values from 0.1 to 1.9
- state_in_weight: bfloat16 [3072, 1024], P('sp', 'tp'), may hold values from -0.109375 to 0.109375
- pool_in_weight: bfloat16 [3072, 1024], P('sp', 'tp'), may hold values from -0.109375 to 0.109375
- rate_real: float32 [64, 64], replicated, may hold values from -1.5 to -0.5
- rate_imag: float32 [64, 64], replicated, may hold values from 0 to 200
- log_step: float32 [64], replicated, may hold values from -2 to 0.7
- input_real: float32 [64, 64, 16], replicated, may hold values from -1 to 1
- input_imag: float32 [64, 64, 16], replicated, may hold values from -1 to 1
- output_real: float32 [64, 16, 64], replicated, may hold values from -64 to 64
- output_imag: float32 [64, 16, 64], replicated, may hold values from -64 to 64
- skip_gain: float32 [1024], replicated, may hold values from -3 to 3
- pool_weight: bfloat16 [16, 64, 64], replicated, may hold values from -0.75 to 0.75
- pool_gain: float32 [1024], replicated, may hold values from 0.1 to 1.9
- state_out_weight: bfloat16 [1024, 3072], P('sp', 'tp'), may hold values from -0.125 to 0.125
- pool_out_weight: bfloat16 [1024, 3072], P('sp', 'tp'), may hold values from -0.125 to 0.125
Outputs:
- mixer_output: bfloat16 [2048, 3072], P('sp', 'tp')
All inputs are finite; a program needn't handle non-finite values.
Results may differ from a plain program's by a relative error of at most 0.0065.
Values may be sent and summed in bfloat16 or wider, within the bound.
A program may use at most 64 MiB of HBM per device.

v0:
```python
import jax
import jax.numpy as jnp
from jax import lax
from jax.sharding import PartitionSpec as P

SSM_GROUP = 16
POOL_GROUP = 64
epsilon = 1e-06
highest = lax.Precision.HIGHEST
window_reach = 16


def prefix(part, axis, combine, identity):
    place = lax.axis_index(axis)
    gathered = jax.tree.map(lambda a: lax.all_gather(a, axis), part)
    state = jax.tree.map(lambda a, e: jnp.zeros_like(a) + jnp.asarray(e, a.dtype), part, identity)

    def one(turn, state):
        return combine(
            state, jax.tree.map(lambda a: lax.dynamic_index_in_dim(a, turn, 0, False), gathered)
        )

    return lax.fori_loop(0, place, one, state)


def passed_along(value, axis, steps):
    count = lax.axis_size(axis)
    first, last = (max(0, -steps), min(count, count - steps))
    return lax.ppermute(value, axis, [(source, source + steps) for source in range(first, last)])


def discretize(rate_real, rate_imag, log_step, length):
    step_size = jnp.exp(log_step)[:, None] / length
    exponent = rate_real * step_size
    angle = rate_imag * step_size
    magnitude = jnp.exp(exponent)
    decay_real = magnitude * jnp.cos(angle)
    decay_imag = magnitude * jnp.sin(angle)
    less_one = jnp.expm1(exponent) * jnp.cos(angle) - 2.0 * jnp.square(jnp.sin(0.5 * angle))
    denominator = rate_real * rate_real + rate_imag * rate_imag
    factor_real = (less_one * rate_real + decay_imag * rate_imag) / denominator
    factor_imag = (decay_imag * rate_real - less_one * rate_imag) / denominator
    return (exponent, angle, decay_real, decay_imag, factor_real, factor_imag)


def complex_product(left_pair, right_pair):
    return jnp.stack(
        [
            left_pair[0] * right_pair[0] - left_pair[1] * right_pair[1],
            left_pair[0] * right_pair[1] + left_pair[1] * right_pair[0],
        ]
    )


def scan_combine(first_part, second_part):
    first_decay_real, first_decay_imag, first_real, first_imag = first_part
    second_decay_real, second_decay_imag, second_real, second_imag = second_part
    return (
        first_decay_real * second_decay_real - first_decay_imag * second_decay_imag,
        first_decay_real * second_decay_imag + first_decay_imag * second_decay_real,
        second_decay_real * first_real - second_decay_imag * first_imag + second_real,
        second_decay_real * first_imag + second_decay_imag * first_real + second_imag,
    )


def chain_combine(earlier, later):
    return (complex_product(later[0], earlier[0]), complex_product(later[0], earlier[1]) + later[1])


def local_slice(array, first_index, count_here):
    return lax.dynamic_slice_in_dim(array, first_index, count_here, 0)


def body(
    tokens,
    norm_gain,
    state_in_weight,
    pool_in_weight,
    rate_real,
    rate_imag,
    log_step,
    input_real,
    input_imag,
    output_real,
    output_imag,
    skip_gain,
    pool_weight,
    pool_gain,
    state_out_weight,
    pool_out_weight,
):
    state_in_full, pool_in_full, state_out_full, pool_out_full = (
        lax.all_gather(state_in_weight, "sp", axis=0, tiled=True),
        lax.all_gather(pool_in_weight, "sp", axis=0, tiled=True),
        lax.all_gather(state_out_weight, "sp", axis=0, tiled=True),
        lax.all_gather(pool_out_weight, "sp", axis=0, tiled=True),
    )
    row_count = tokens.shape[0]
    model_width = norm_gain.shape[0]
    state_width = state_in_full.shape[1]
    pool_width = pool_in_full.shape[1]
    features = lax.all_gather(tokens, "tp", axis=1, tiled=True).astype(jnp.float32)
    scaled = (features * norm_gain).astype(jnp.bfloat16)
    state_rows = state_in_full
    pool_rows = pool_in_full
    state_sum = jnp.dot(scaled, state_rows, preferred_element_type=jnp.float32)
    pool_sum = jnp.dot(scaled, pool_rows, preferred_element_type=jnp.float32)
    squares = jnp.sum(features * features, axis=1)
    state_sum, pool_sum, squares = (state_sum, pool_sum, squares)
    inverse = lax.rsqrt(squares / model_width + epsilon)[:, None]
    state_in = (state_sum * inverse).astype(jnp.bfloat16)
    pool_in = (pool_sum * inverse).astype(jnp.bfloat16)
    head_index = lax.axis_index("tp")
    block_index = lax.axis_index("sp")
    groups_here = state_width // SSM_GROUP
    first_group = head_index * groups_here
    length = row_count * lax.axis_size("sp")
    exponent, angle, decay_real, decay_imag, factor_real, factor_imag = discretize(
        local_slice(rate_real, first_group, groups_here),
        local_slice(rate_imag, first_group, groups_here),
        local_slice(log_step, first_group, groups_here),
        length,
    )
    state_columns = groups_here * decay_real.shape[1]
    exponent = exponent.reshape(state_columns)
    angle = angle.reshape(state_columns)
    decay_real = decay_real.reshape(state_columns)
    decay_imag = decay_imag.reshape(state_columns)
    group_identity = jnp.eye(groups_here, dtype=jnp.float32)
    local_in_real = local_slice(input_real, first_group, groups_here)
    local_in_imag = local_slice(input_imag, first_group, groups_here)
    drive_real = factor_real[..., None] * local_in_real - factor_imag[..., None] * local_in_imag
    drive_imag = factor_real[..., None] * local_in_imag + factor_imag[..., None] * local_in_real
    drive_matrix_real = jnp.einsum("gnc,gh->gchn", drive_real, group_identity).reshape(
        state_width, state_columns
    )
    drive_matrix_imag = jnp.einsum("gnc,gh->gchn", drive_imag, group_identity).reshape(
        state_width, state_columns
    )
    signal = state_in.astype(jnp.float32)
    push_real = jnp.dot(signal, drive_matrix_real, precision=highest)
    push_imag = jnp.dot(signal, drive_matrix_imag, precision=highest)
    decay_wide_real = jnp.broadcast_to(decay_real, push_real.shape)
    decay_wide_imag = jnp.broadcast_to(decay_imag, push_real.shape)
    _, _, local_real, local_imag = lax.associative_scan(
        scan_combine, (decay_wide_real, decay_wide_imag, push_real, push_imag), axis=0
    )
    end_state = jnp.stack([local_real[row_count - 1], local_imag[row_count - 1]])
    block_magnitude = jnp.exp(row_count * exponent)
    block_decay = jnp.stack(
        [block_magnitude * jnp.cos(row_count * angle), block_magnitude * jnp.sin(row_count * angle)]
    )
    last_rows = pool_in[row_count - window_reach :]
    identity = (
        jnp.stack([jnp.ones_like(exponent), jnp.zeros_like(exponent)]),
        jnp.zeros_like(end_state),
    )
    _, incoming = prefix((block_decay, end_state), "sp", chain_combine, identity)
    halo_block = passed_along(last_rows, "sp", 1)
    positions = (jnp.arange(row_count, dtype=jnp.float32) + 1.0)[:, None]
    power_magnitude = jnp.exp(positions * exponent[None, :])
    power_angle = positions * angle[None, :]
    power_cos = power_magnitude * jnp.cos(power_angle)
    power_sin = power_magnitude * jnp.sin(power_angle)
    states_real = local_real + power_cos * incoming[0] - power_sin * incoming[1]
    states_imag = local_imag + power_cos * incoming[1] + power_sin * incoming[0]
    local_out_real = local_slice(output_real, first_group, groups_here)
    local_out_imag = local_slice(output_imag, first_group, groups_here)
    read_matrix_real = jnp.einsum("gcn,gh->hngc", local_out_real, group_identity).reshape(
        state_columns, state_width
    )
    read_matrix_imag = jnp.einsum("gcn,gh->hngc", local_out_imag, group_identity).reshape(
        state_columns, state_width
    )
    readout_sum = jnp.dot(states_real, read_matrix_real, precision=highest)
    readout_sum = readout_sum - jnp.dot(states_imag, read_matrix_imag, precision=highest)
    readout_sum = (
        readout_sum + local_slice(skip_gain, head_index * state_width, state_width) * signal
    )
    state_out = jax.nn.gelu(readout_sum).astype(jnp.bfloat16)
    pool_groups_here = pool_width // POOL_GROUP
    first_pool = head_index * pool_groups_here
    extended = jnp.concatenate([halo_block, pool_in], axis=0)
    column_group = first_pool + jnp.arange(pool_width, dtype=jnp.int32) // POOL_GROUP
    column_window = jnp.left_shift(jnp.ones_like(column_group), column_group % 4 + 1)
    targets = jnp.arange(row_count, dtype=jnp.int32)[:, None] + window_reach
    sources = jnp.arange(row_count + window_reach, dtype=jnp.int32)[None, :]
    window_sums = jnp.zeros((row_count, pool_width), jnp.float32)
    for power_index in range(1, 5):
        span_width = 2**power_index
        band_mask = ((sources <= targets) & (sources > targets - span_width)).astype(jnp.bfloat16)
        partial_sums = jnp.dot(band_mask, extended, preferred_element_type=jnp.float32)
        window_sums = jnp.where(column_window[None, :] == span_width, partial_sums, window_sums)
    global_rows = block_index * row_count + jnp.arange(row_count, dtype=jnp.int32)
    divisor = jnp.minimum(global_rows[:, None] + 1, column_window[None, :]).astype(jnp.float32)
    pooled = window_sums / divisor - pool_in.astype(jnp.float32)
    pool_identity = jnp.eye(pool_groups_here, dtype=jnp.float32)
    mixer_matrix = jnp.einsum(
        "gcd,gh->gchd",
        local_slice(pool_weight, first_pool, pool_groups_here).astype(jnp.float32),
        pool_identity,
    ).reshape(pool_width, pool_width)
    projected = jnp.dot(pooled, mixer_matrix, precision=highest)
    pool_out = (projected * local_slice(pool_gain, head_index * pool_width, pool_width)).astype(
        jnp.bfloat16
    )
    state_rows = state_out_full
    pool_rows = pool_out_full
    running_sum = jnp.dot(
        lax.all_gather(state_out, "tp", axis=1, tiled=True),
        state_rows,
        preferred_element_type=jnp.float32,
    )
    combined = running_sum + jnp.dot(
        lax.all_gather(pool_out, "tp", axis=1, tiled=True),
        pool_rows,
        preferred_element_type=jnp.float32,
    )
    return combined.astype(jnp.bfloat16)


def solution(mesh):
    return jax.shard_map(
        body,
        mesh=mesh,
        in_specs=(
            P("sp", "tp"),
            P(),
            P("sp", "tp"),
            P("sp", "tp"),
            P(),
            P(),
            P(),
            P(),
            P(),
            P(),
            P(),
            P(),
            P(),
            P(),
            P("sp", "tp"),
            P("sp", "tp"),
        ),
        out_specs=P("sp", "tp"),
        check_vma=False,
    )
```

profile of v0, /device:TPU:25, one launch (start us, length us, event | category | flops | bytes accessed | tf_op | source)
XLA Modules:
  0.0 252.3 jit_solution(12776405410376965267)
XLA Ops:
  18.1 1.9 multiply_bitcast_fusion
  20.0 2.8 %reshape.307 = f32[1024,256]{0,1:T(8,128)} reshape(f32[16,64,16,16]{1,0,3,2:T(8,128)} %get-tuple-element.121) | data formatting | bytes 2097152 | tf_op jit(solution)/shard_map/reshape | solution.py:169
  23.8 2.6 %multiply_bitcast_fusion.2 = (f32[16,16,16,64]{3,2,1,0:T(8,128)}, f32[16,16,16,64]{3,2,1,0:T(8,128)}) fusion(f32[16,64,16]{1,2,0:T(8,128)S(1)} %get-tuple-element.81, f32[16,16]{1,0:T(8,128)S(1)} %fusion.78, f32[16,64,16]{1,2,0:T(8,128)S(1)} %get-tuple-element.82), kind=kLoop, calls=%fused_computation.11 | loop fusion | flops 524288 | bytes 2229248 | tf_op jit(solution)/shard_map/gnc,gh->gchn/transpose | solution.py:137
  26.3 2.0 reshape.306
  28.5 2.8 %reshape.303 = f32[256,1024]{1,0:T(8,128)} reshape(f32[16,16,16,64]{3,2,1,0:T(8,128)} %get-tuple-element.127) | data formatting | bytes 2097152 | tf_op jit(solution)/shard_map/reshape | solution.py:134
  32.8 23.6 %all-gather.2 = f32[8,2,1024]{2,1,0:T(2,128)} all-gather(f32[1,2,1024]{2,1,0:T(2,128)S(1)} %maximum_bitcast_fusion), channel_id=2, replica_groups=mesh['sp'=8,'tp'=4] {'sp'}, dimensions={0}, use_global_device_ids=true | all-gather | bytes 73728 | tf_op jit(solution)/shard_map/all_gather | solution.py:15
  56.3 1.5 reshape.308
  65.0 1.9 fusion.1
  67.0 7.2 %all-gather.12.cloned.1.call-done = bf16[3072,256]{1,0:T(8,128)(2,1)} async-done(((bf16[384,256]{1,0:T(8,128)(2,1)}), bf16[3072,256]{1,0:T(8,128)(2,1)}) %all-gather.12.cloned.1.call-update) | async-done | bytes 1572880 | tf_op jit(solution)/shard_map/all_gather | solution.py:93
  74.2 2.0 fusion.20
  76.9 1.5 slice.477
  78.4 1.5 slice.389
  79.9 1.5 slice.382
  82.1 1.6 slice.380
  83.6 1.5 slice.383
  85.1 1.8 add_add_fusion.1
  90.0 2.0 add_add_fusion.3
  94.1 1.6 slice.395
  95.7 1.6 slice.399
  97.3 1.8 add_add_fusion.5
  100.4 1.5 slice.403
  102.0 1.5 slice.407
  103.5 1.6 add_add_fusion.7
  105.1 1.5 slice.454
  106.6 1.5 slice.421
  108.0 1.4 slice.414
  109.5 1.5 slice.411
  110.9 1.5 slice.415
  112.4 1.5 add_add_fusion.9
  119.3 1.4 add_add_fusion.11
  126.1 1.5 slice_add_fusion.14
  133.0 1.5 slice.450
  137.8 1.6 slice.456
  146.0 1.6 slice.474
  156.6 2.7 %pad.126 = f32[256,1024]{1,0:T(8,128)} pad(f32[128,1024]{1,0:T(8,128)S(1)} %pad_maximum_fusion, f32[]{:T(128)} %constant.91.clone.1), padding=0_1_1x0_0_0 | pad | bytes 1572868 | tf_op jit(solution)/shard_map/pad | solution.py:145
  159.4 2.7 %pad.127 = f32[256,1024]{1,0:T(8,128)} pad(f32[128,1024]{1,0:T(8,128)S(1)} %add.689, f32[]{:T(128)} %constant.91.clone.1), padding=1_0_1x0_0_0 | pad | bytes 1572868 | tf_op jit(solution)/shard_map/pad | solution.py:145
  162.1 2.7 %pad.129 = f32[256,1024]{1,0:T(8,128)} pad(f32[128,1024]{1,0:T(8,128)S(1)} %add.692, f32[]{:T(128)} %constant.91.clone.1), padding=1_0_1x0_0_0 | pad | bytes 1572868 | tf_op jit(solution)/shard_map/pad | solution.py:145
  164.9 2.7 %pad.128 = f32[256,1024]{1,0:T(8,128)} pad(f32[128,1024]{1,0:T(8,128)S(1)} %pad_maximum_fusion.1, f32[]{:T(128)} %constant.91.clone.1), padding=0_1_1x0_0_0 | pad | bytes 1572868 | tf_op jit(solution)/shard_map/pad | solution.py:145
  169.2 22.5 %all-gather.3 = f32[8,2,1024]{2,1,0:T(2,128)S(1)} all-gather(f32[1,2,1024]{2,1,0:T(2,128)S(1)} %maximum_bitcast_fusion.1), channel_id=3, replica_groups=mesh['sp'=8,'tp'=4] {'sp'}, dimensions={0}, use_global_device_ids=true | all-gather | bytes 73728 | tf_op jit(solution)/shard_map/all_gather | solution.py:15
  191.6 5.0 %while.12 = (s32[]{:T(128)}, f32[2,1024]{1,0:T(2,128)S(1)}, s32[]{:T(128)}, f32[8,2,1024]{2,1,0:T(2,128)}, f32[8,2,1024]{2,1,0:T(2,128)S(1)}, /*index=5*/s32[]{:T(128)}, s32[]{:T(128)}, s32[]{:T(128)}, s32[]{}) while((s32[]{:T(128)}, f32[2,1024]{1,0:T(2,128)S(1)}, s32[]{:T(128)}, f32[8,2,1024]{2,1,0:T(2,128)}, f32[8,2,1024]{2,1,0:T(2,128)S(1)}, ...), condition=%wide.region_2.3_spmd, body=%wide.region_1.2_spmd.sunk | while | flops 10246 | bytes 49311 | solution.py:23
  196.8 2.1 fusion.17
  199.0 5.8 %collective-permute-start = (bf16[16,256]{1,0:T(8,128)(2,1)S(1)}, bf16[16,256]{1,0:T(8,128)(2,1)S(1)}, u32[]{:S(2)}, u32[]{:S(2)}) collective-permute-start(bf16[16,256]{1,0:T(8,128)(2,1)S(1)} %slice.534), channel_id=1, source_target_pairs={{0,4},{4,8},{8,12},{12,16},{16,20},{20,24},{24,28},{1,5},{5,9},{9,... | collective-permute-start | bytes 24584 | tf_op jit(solution)/shard_map/ppermute | solution.py:29
  204.9 5.1 %fusion.29 = f32[256,256]{1,0:T(8,128)S(1)} fusion(f32[1024,256]{0,1:T(8,128)S(1)} %copy-done.12, f32[256,1024]{1,0:T(8,128)S(1)} %copy-done.9, f32[256,1024]{1,0:T(8,128)S(1)} %copy-done.11, f32[1024]{0:T(1024)S(1)} %bitcast.64, f32[1024]{0:T(1024)S(1)} %bitcast.62, f32[1024]{0:T(1024)S(1)} %copy-done.52, f32[1024]{0:T(1024)S(1)} %copy-done.53, ...), kind=kOutput, calls=%fused_computation.39 | convolution fusion | flops 807665664 | bytes 3425280 | tf_op jit(solution)/shard_map/dot_general | solution.py:175
  210.0 5.1 %fusion.67 = bf16[256,256]{1,0:T(8,128)(2,1)S(1)} fusion(f32[256,256]{1,0:T(8,128)S(1)} %fusion.29, f32[1024,256]{0,1:T(8,128)S(1)} %copy-done.13, f32[256,1024]{1,0:T(8,128)S(1)} %copy-done.10, f32[256,1024]{1,0:T(8,128)S(1)} %copy-done.8, f32[1024]{0:T(1024)S(1)} %bitcast.65, f32[1024]{0:T(1024)S(1)} %bitcast.63, f32[1024]{0:T(1024)S(1)} %copy-done.52, ...), kind=kOutput, calls=%fused_computation.83 | convolution fusion | flops 808517632 | bytes 3688448 | tf_op jit(solution)/shard_map/dot_general | solution.py:176
  215.2 16.8 %all_gather.39 = bf16[256,1024]{1,0:T(8,128)(2,1)S(1)} all-gather(bf16[256,256]{1,0:T(8,128)(2,1)S(1)} %fusion.67), channel_id=1, replica_groups=mesh['sp'=8,'tp'=4] {'tp'}, dimensions={1}, use_global_device_ids=true | all-gather | bytes 655360 | tf_op jit(solution)/shard_map/all_gather | solution.py:210
  232.1 2.0 fusion.93
  235.8 7.3 %all_gather.42 = bf16[256,1024]{1,0:T(8,128)(2,1)S(1)} all-gather(bf16[256,256]{1,0:T(8,128)(2,1)S(1)} %fusion.16), channel_id=1, replica_groups=mesh['sp'=8,'tp'=4] {'tp'}, dimensions={1}, use_global_device_ids=true | all-gather | bytes 655360 | tf_op jit(solution)/shard_map/all_gather | solution.py:215
  243.1 2.7 %fusion.6 = bf16[256,768]{1,0:T(8,128)(2,1)} fusion(f32[256,768]{1,0:T(8,128)S(1)} %fusion.93, bf16[256,1024]{1,0:T(8,128)(2,1)S(1)} %all_gather.42, bf16[1024,768]{1,0:T(8,128)(2,1)} %all-gather.18.cloned.1.call-done), kind=kOutput, calls=%fused_computation.18 | convolution fusion | flops 403046400 | bytes 3276800 | tf_op jit(solution)/shard_map/dot_general | solution.py:214
  (307 shorter events, 72.0 us)
Async XLA Ops:
  6.5 58.5 %all-gather.10.cloned.1.call-start = ((), (), s32[]{:S(2)}) async-start(), calls=%async_computation | async-start | bytes 1966080 | tf_op jit(solution)/shard_map/all_gather | solution.py:102
  7.3 66.9 %all-gather.12.cloned.1.call-start = ((), (), s32[]{:S(2)}) async-start(), calls=%async_computation.1 | async-start | bytes 1769472 | tf_op jit(solution)/shard_map/all_gather | solution.py:93
  8.0 188.7 %all-gather.16.cloned.1.call-start = ((), (), s32[]{:S(2)}) async-start(), calls=%async_computation.3 | async-start | bytes 1769472 | tf_op jit(solution)/shard_map/all_gather | solution.py:94
  8.7 223.3 %all-gather.14.cloned.1.call-start = ((), (), s32[]{:S(2)}) async-start(), calls=%async_computation.2 | async-start | bytes 1769472 | tf_op jit(solution)/shard_map/all_gather | solution.py:95
  9.3 233.7 %all-gather.18.cloned.1.call-start = ((), (), s32[]{:S(2)}) async-start(), calls=%async_computation.4 | async-start | bytes 1769472 | tf_op jit(solution)/shard_map/all_gather | solution.py:96
  28.4 56.7 %copy-start.25 = (f32[1024]{0:T(1024)}, f32[1024]{0:T(1024)S(1)}, u32[]{:S(2)}) copy-start(f32[1024]{0:T(1024)S(1)} %reshape.305) | copy-start | bytes 12292
  28.5 56.7 %copy-start.27 = (f32[1024]{0:T(1024)}, f32[1024]{0:T(1024)S(1)}, u32[]{:S(2)}) copy-start(f32[1024]{0:T(1024)S(1)} %reshape.304) | copy-start | bytes 12292
  59.3 14.8 %copy-start.61 = (f32[3072]{0:T(1024)S(1)}, f32[3072]{0:T(1024)}, u32[]{:S(2)}) copy-start(f32[3072]{0:T(1024)} %param.19) | copy-start | bytes 36868
  63.9 26.2 %copy-start.29 = (f32[1024]{0:T(1024)}, f32[1024]{0:T(1024)S(1)}, u32[]{:S(2)}) copy-start(f32[1024]{0:T(1024)S(1)} %get-tuple-element.72) | copy-start | bytes 12292
  63.9 26.2 %copy-start.31 = (f32[1024]{0:T(1024)}, f32[1024]{0:T(1024)S(1)}, u32[]{:S(2)}) copy-start(f32[1024]{0:T(1024)S(1)} %get-tuple-element.73) | copy-start | bytes 12292
  63.9 33.5 %copy-start.33 = (f32[1024]{0:T(1024)}, f32[1024]{0:T(1024)S(1)}, u32[]{:S(2)}) copy-start(f32[1024]{0:T(1024)S(1)} %get-tuple-element.70) | copy-start | bytes 12292
  63.9 33.5 %copy-start.35 = (f32[1024]{0:T(1024)}, f32[1024]{0:T(1024)S(1)}, u32[]{:S(2)}) copy-start(f32[1024]{0:T(1024)S(1)} %get-tuple-element.71) | copy-start | bytes 12292
  63.9 39.6 %copy-start.37 = (f32[1024]{0:T(1024)}, f32[1024]{0:T(1024)S(1)}, u32[]{:S(2)}) copy-start(f32[1024]{0:T(1024)S(1)} %get-tuple-element.68) | copy-start | bytes 12292
  63.9 39.6 %copy-start.39 = (f32[1024]{0:T(1024)}, f32[1024]{0:T(1024)S(1)}, u32[]{:S(2)}) copy-start(f32[1024]{0:T(1024)S(1)} %get-tuple-element.69) | copy-start | bytes 12292
  65.0 9.1 %copy-start.6 = (bf16[256,3072]{1,0:T(8,128)(2,1)S(1)}, bf16[256,3072]{1,0:T(8,128)(2,1)}, u32[]{:S(2)}) copy-start(bf16[256,3072]{1,0:T(8,128)(2,1)} %all-gather.10.cloned.1.call-done) | copy-start | bytes 4718596
  67.0 9.2 %copy-start.59 = (f32[256]{0:T(256)}, f32[256]{0:T(256)S(1)}, u32[]{:S(2)}) copy-start(f32[256]{0:T(256)S(1)} %add_rsqrt_fusion) | copy-start | bytes 3076
  76.2 5.2 %copy-start.16 = (bf16[256,256]{1,0:T(8,128)(2,1)}, bf16[256,256]{1,0:T(8,128)(2,1)S(1)}, u32[]{:S(2)}) copy-start(bf16[256,256]{1,0:T(8,128)(2,1)S(1)} %fusion.20) | copy-start | bytes 393220
  76.9 70.7 %copy-start = (f32[256,1024]{1,0:T(8,128)}, f32[256,1024]{1,0:T(8,128)S(1)}, u32[]{:S(2)}) copy-start(f32[256,1024]{1,0:T(8,128)S(1)} %fusion.92) | copy-start | bytes 3145732
  76.9 4.5 %copy-start.2 = (f32[256,1024]{1,0:T(8,128)S(1)}, f32[256,1024]{1,0:T(8,128)}, u32[]{:S(2)}) copy-start(f32[256,1024]{1,0:T(8,128)} %reshape.303) | copy-start | bytes 3145732
  82.0 65.5 %copy-start.1 = (f32[256,1024]{1,0:T(8,128)}, f32[256,1024]{1,0:T(8,128)S(1)}, u32[]{:S(2)}) copy-start(f32[256,1024]{1,0:T(8,128)S(1)} %fusion.91) | copy-start | bytes 3145732
  145.9 5.5 %copy-start.50 = (f32[1,1024]{1,0:T(1,128)S(1)}, f32[1,1024]{1,0:T(1,128)}, u32[]{:S(2)}) copy-start(f32[1,1024]{1,0:T(1,128)} %slice.506) | copy-start | bytes 12292
  145.9 5.6 %copy-start.21 = (f32[7,1024]{1,0:T(8,128)S(1)}, f32[7,1024]{1,0:T(8,128)}, u32[]{:S(2)}) copy-start(f32[7,1024]{1,0:T(8,128)} %slice.454) | copy-start | bytes 86020
  145.9 5.6 %copy-start.22 = (f32[7,1024]{1,0:T(8,128)S(1)}, f32[7,1024]{1,0:T(8,128)}, u32[]{:S(2)}) copy-start(f32[7,1024]{1,0:T(8,128)} %slice.450) | copy-start | bytes 86020
  145.9 5.6 %copy-start.41 = (f32[1024]{0:T(1024)S(1)}, f32[1024]{0:T(1024)}, u32[]{:S(2)}) copy-start(f32[1024]{0:T(1024)} %get-tuple-element.66) | copy-start | bytes 12292
  145.9 5.6 %copy-start.42 = (f32[1024]{0:T(1024)S(1)}, f32[1024]{0:T(1024)}, u32[]{:S(2)}) copy-start(f32[1024]{0:T(1024)} %get-tuple-element.67) | copy-start | bytes 12292
  145.9 5.6 %copy-start.49 = (f32[1,1024]{1,0:T(1,128)S(1)}, f32[1,1024]{1,0:T(1,128)}, u32[]{:S(2)}) copy-start(f32[1,1024]{1,0:T(1,128)} %slice.486) | copy-start | bytes 12292
  145.9 5.8 %copy-start.48 = (f32[1,1024]{1,0:T(1,128)S(1)}, f32[1,1024]{1,0:T(1,128)}, u32[]{:S(2)}) copy-start(f32[1,1024]{1,0:T(1,128)} %slice.511) | copy-start | bytes 12292
  145.9 5.8 %copy-start.19 = (f32[15,1024]{1,0:T(8,128)S(1)}, f32[15,1024]{1,0:T(8,128)}, u32[]{:S(2)}) copy-start(f32[15,1024]{1,0:T(8,128)} %slice.460) | copy-start | bytes 184324
  145.9 5.8 %copy-start.20 = (f32[15,1024]{1,0:T(8,128)S(1)}, f32[15,1024]{1,0:T(8,128)}, u32[]{:S(2)}) copy-start(f32[15,1024]{1,0:T(8,128)} %slice.456) | copy-start | bytes 184324
  145.9 5.8 %copy-start.38 = (f32[1024]{0:T(1024)S(1)}, f32[1024]{0:T(1024)}, u32[]{:S(2)}) copy-start(f32[1024]{0:T(1024)} %copy-done.37) | copy-start | bytes 12292
  146.0 5.8 %copy-start.40 = (f32[1024]{0:T(1024)S(1)}, f32[1024]{0:T(1024)}, u32[]{:S(2)}) copy-start(f32[1024]{0:T(1024)} %copy-done.39) | copy-start | bytes 12292
  159.4 5.4 %slice-start = ((f32[256,1024]{1,0:T(8,128)}), f32[1,1024]{1,0:T(1,128)S(1)}, s32[]{:S(2)}) async-start(f32[256,1024]{1,0:T(8,128)} %copy-done), calls=%async_computation.5 | async-start | bytes 8192 | tf_op jit(solution)/shard_map/slice | solution.py:145
  159.4 5.4 %copy-start.5 = (f32[127,1024]{1,0:T(8,128)S(1)}, f32[127,1024]{1,0:T(8,128)}, u32[]{:S(2)}) copy-start(f32[127,1024]{1,0:T(8,128)} %get-tuple-element.79) | copy-start | bytes 1560580
  164.8 31.9 %copy-start.7 = (bf16[256,3072]{1,0:T(8,128)(2,1)S(1)}, bf16[256,3072]{1,0:T(8,128)(2,1)}, u32[]{:S(2)}) copy-start(bf16[256,3072]{1,0:T(8,128)(2,1)} %all-gather.10.cloned.1.call-done) | copy-start | bytes 4718596
  164.8 32.0 %copy-start.60 = (f32[256]{0:T(256)S(1)}, f32[256]{0:T(256)}, u32[]{:S(2)}) copy-start(f32[256]{0:T(256)} %copy-done.59) | copy-start | bytes 3076
  164.8 32.0 %copy-start.62 = (f32[3072]{0:T(1024)S(1)}, f32[3072]{0:T(1024)}, u32[]{:S(2)}) copy-start(f32[3072]{0:T(1024)} %param.19) | copy-start | bytes 36868
  196.7 8.1 %copy-start.9 = (f32[256,1024]{1,0:T(8,128)S(1)}, f32[256,1024]{1,0:T(8,128)}, u32[]{:S(2)}) copy-start(f32[256,1024]{1,0:T(8,128)} %pad.126) | copy-start | bytes 3145732
  196.7 8.1 %copy-start.52 = (f32[1024]{0:T(1024)S(1)}, f32[1024]{0:T(1024)}, u32[]{:S(2)}) copy-start(f32[1024]{0:T(1024)} %mul.1012) | copy-start | bytes 12292
  196.7 8.1 %copy-start.53 = (f32[1024]{0:T(1024)S(1)}, f32[1024]{0:T(1024)}, u32[]{:S(2)}) copy-start(f32[1024]{0:T(1024)} %mul.1009) | copy-start | bytes 12292
  196.7 8.1 %copy-start.69 = (f32[256]{0:T(256)S(1)}, f32[256]{0:T(256)}, u32[]{:S(2)}) copy-start(f32[256]{0:T(256)} %iota_add_fusion.4) | copy-start | bytes 3076
  196.8 8.1 %copy-start.11 = (f32[256,1024]{1,0:T(8,128)S(1)}, f32[256,1024]{1,0:T(8,128)}, u32[]{:S(2)}) copy-start(f32[256,1024]{1,0:T(8,128)} %pad.127) | copy-start | bytes 3145732
  196.8 8.1 %copy-start.12 = (f32[1024,256]{0,1:T(8,128)S(1)}, f32[1024,256]{0,1:T(8,128)}, u32[]{:S(2)}) copy-start(f32[1024,256]{0,1:T(8,128)} %reshape.307) | copy-start | bytes 3145732
  199.0 35.1 %collective-permute-start = (bf16[16,256]{1,0:T(8,128)(2,1)S(1)}, bf16[16,256]{1,0:T(8,128)(2,1)S(1)}, u32[]{:S(2)}, u32[]{:S(2)}) collective-permute-start(bf16[16,256]{1,0:T(8,128)(2,1)S(1)} %slice.534), channel_id=1, source_target_pairs={{0,4},{4,8},{8,12},{12,16},{16,20},{20,24},{24,28},{1,5},{5,9},{9,... | collective-permute-start | bytes 24584 | tf_op jit(solution)/shard_map/ppermute | solution.py:29
  204.9 5.1 %copy-start.8 = (f32[256,1024]{1,0:T(8,128)S(1)}, f32[256,1024]{1,0:T(8,128)}, u32[]{:S(2)}) copy-start(f32[256,1024]{1,0:T(8,128)} %pad.129) | copy-start | bytes 3145732
  204.9 5.1 %copy-start.10 = (f32[256,1024]{1,0:T(8,128)S(1)}, f32[256,1024]{1,0:T(8,128)}, u32[]{:S(2)}) copy-start(f32[256,1024]{1,0:T(8,128)} %pad.128) | copy-start | bytes 3145732
  204.9 5.1 %copy-start.13 = (f32[1024,256]{0,1:T(8,128)S(1)}, f32[1024,256]{0,1:T(8,128)}, u32[]{:S(2)}) copy-start(f32[1024,256]{0,1:T(8,128)} %reshape.308) | copy-start | bytes 3145732
  204.9 5.1 %copy-start.17 = (bf16[256,256]{1,0:T(8,128)(2,1)S(1)}, bf16[256,256]{1,0:T(8,128)(2,1)}, u32[]{:S(2)}) copy-start(bf16[256,256]{1,0:T(8,128)(2,1)} %copy-done.16) | copy-start | bytes 393220
  204.9 5.1 %copy-start.58 = (f32[256]{0:T(256)S(1)}, f32[256]{0:T(256)}, u32[]{:S(2)}) copy-start(f32[256]{0:T(256)} %dynamic_slice.46) | copy-start | bytes 3076
  (30 other events, 43.2 us)
Sparse Core Ops, SparseCore 0:
  8.9 21.0 all-gather.9
  32.1 42.0 all-gather.11
  76.4 42.4 all-gather.15
  120.9 42.5 all-gather.13
  165.5 42.8 all-gather.17
where the time goes:
time: 255 us; the launch traced here: 252 us
  local copies, waits for them, and re-layouts  89.1 us (35%)
  blocking collectives  70.1 us (27%)
  other arithmetic  40.2 us (16%)
  matrix products  21.9 us (9%)
  between operations  14.5 us (6%)
  waiting for transfers between devices  10.4 us (4%)
  starting transfers between devices  5.98 us (2%)
    slice x54, local copies, waits for them, and re-layouts, body(): lax.associative_scan(scan_combine, (decay_wide_real, decay_wide_imag, pus...  56.2 us
    all_gather x2, blocking collectives, prefix(): gathered = jax.tree.map(lambda a: lax.all_gather(a, axis), part)  46 us
    all_gather x1, blocking collectives, body(): lax.all_gather(state_out, 'tp', axis=1, tiled=True)  16.8 us
    add x13, other arithmetic, scan_combine(): second_decay_real * first_imag + second_decay_imag * first_real  13.6 us
    pad x28, local copies, waits for them, and re-layouts, body(): lax.associative_scan(scan_combine, (decay_wide_real, decay_wide_imag, pus...  13 us
    all_gather x1, blocking collectives, body(): lax.all_gather(pool_out, 'tp', axis=1, tiled=True)  7.28 us
    all_gather x1, waiting for transfers between devices, body(): lax.all_gather(state_in_weight, 'sp', axis=0, tiled=True)  7.19 us
    ppermute x1, starting transfers between devices, passed_along(): lax.ppermute(value, axis, [(source, source + steps) for source in range(f...  5.83 us
  transfers between devices with their start and end apart: 6, of which 1 were waited for; matrix products, arithmetic and copies ran while one was open for 58% of the time, Pallas kernels for 0%

commit v1 on v0

--- a/solution.py
+++ b/solution.py
@@ -89,6 +89,21 @@
     state_out_weight,
     pool_out_weight,
 ):
+
+    def return_all_the_tokens(original):
+        z2, wide_out, carry_out = (
+            jax.lax.axis_size("tp"),
+            jax.lax.axis_index("tp"),
+            original.shape[1],
+        )
+        val, met_up = (original, 1)
+        while met_up < z2:
+            val = jnp.concatenate(
+                [val, jax.lax.ppermute(val, "tp", [(s, (s - met_up) % z2) for s in range(z2)])], 1
+            )
+            met_up = 2 * met_up
+        return jnp.roll(val, wide_out * carry_out, 1)
+
     state_in_full, pool_in_full, state_out_full, pool_out_full = (
         lax.all_gather(state_in_weight, "sp", axis=0, tiled=True),
         lax.all_gather(pool_in_weight, "sp", axis=0, tiled=True),
@@ -207,9 +222,7 @@
     state_rows = state_out_full
     pool_rows = pool_out_full
     running_sum = jnp.dot(
-        lax.all_gather(state_out, "tp", axis=1, tiled=True),
-        state_rows,
-        preferred_element_type=jnp.float32,
+        return_all_the_tokens(state_out), state_rows, preferred_element_type=jnp.float32
     )
     combined = running_sum + jnp.dot(
         lax.all_gather(pool_out, "tp", axis=1, tiled=True),

time: 255 us -> 223 us (0.87)
  local copies, waits for them, and re-layouts: 89.1 us -> 41.1 us
  waiting for transfers between devices: 10.4 us -> 38.7 us
  blocking collectives: 70.1 us -> 54.2 us
  other arithmetic: 40.2 us -> 29.3 us
  matrix products: 21.9 us -> 29.4 us
  starting transfers between devices: 5.98 us -> 12.3 us
    slice x54, local copies, waits for them, and re-layouts: 56.2 us -> 14.4 us  [body(): lax.associative_scan(scan_combine, (decay_wide_real, decay_wide_imag, pus...]
    all_gather x1, waiting for transfers between devices: 0.02 us -> 20.1 us  [body(): lax.all_gather(pool_in_weight, 'sp', axis=0, tiled=True)]
    all_gather x1 -> x0, blocking collectives: 16.8 us -> none  [body(): lax.all_gather(state_out, 'tp', axis=1, tiled=True)]
    ppermute x0 -> x2, starting transfers between devices: none -> 9.69 us  [return_all_the_tokens(): jax.lax.ppermute(val, 'tp', [(s, (s - met_up) % z2) for s in range(z2)])]
    add x13, other arithmetic: 13.6 us -> 5.89 us  [scan_combine(): second_decay_real * first_imag + second_decay_imag * first_real]
    ppermute x0 -> x2, waiting for transfers between devices: none -> 4.5 us  [return_all_the_tokens(): jax.lax.ppermute(val, 'tp', [(s, (s - met_up) % z2) for s in range(z2)])]
    pad x28, local copies, waits for them, and re-layouts: 13 us -> 8.95 us  [body(): lax.associative_scan(scan_combine, (decay_wide_real, decay_wide_imag, pus...]
    dot_general x4, matrix products: 1.13 us -> 4.9 us  [body(): jnp.dot(band_mask, extended, preferred_element_type=jnp.float32)]
  transfers between devices with their start and end apart: 6 -> 8, of which waited for: 1 -> 3; matrix products, arithmetic and copies ran while one was open for 58% -> 43% of each run, Pallas kernels for 0% -> 0%
where the time goes in v1:
time: 223 us; the launch traced here: 220 us
  blocking collectives  54.2 us (24%)
  local copies, waits for them, and re-layouts  41.1 us (18%)
  waiting for transfers between devices  38.7 us (17%)
  matrix products  29.4 us (13%)
  other arithmetic  29.3 us (13%)
  between operations  14.5 us (7%)
  starting transfers between devices  12.3 us (6%)
    all_gather x2, blocking collectives, prefix(): gathered = jax.tree.map(lambda a: lax.all_gather(a, axis), part)  46.9 us
    all_gather x1, waiting for transfers between devices, body(): lax.all_gather(pool_in_weight, 'sp', axis=0, tiled=True)  20.1 us
    slice x54, local copies, waits for them, and re-layouts, body(): lax.associative_scan(scan_combine, (decay_wide_real, decay_wide_imag, pus...  14.4 us
    all_gather x1, waiting for transfers between devices, body(): lax.all_gather(state_in_weight, 'sp', axis=0, tiled=True)  10.9 us
    ppermute x2, starting transfers between devices, return_all_the_tokens(): jax.lax.ppermute(val, 'tp', [(s, (s - met_up) % z2) for s in range(z2)])  9.69 us
    pad x28, local copies, waits for them, and re-layouts, body(): lax.associative_scan(scan_combine, (decay_wide_real, decay_wide_imag, pus...  8.95 us
    dot_general x1, matrix products, body(): readout_sum = jnp.dot(states_real, read_matrix_real, precision=highest)  7.75 us
    all_gather x1, blocking collectives, body(): lax.all_gather(pool_out, 'tp', axis=1, tiled=True)  7.28 us
  transfers between devices with their start and end apart: 8, of which 3 were waited for; matrix products, arithmetic and copies ran while one was open for 43% of the time, Pallas kernels for 0%

profile of v1, /device:TPU:25, one launch (start us, length us, event | category | flops | bytes accessed | tf_op | source)
XLA Modules:
  0.0 219.7 jit_solution(10877835517567969461)
XLA Ops:
  14.0 0.8 cosine_multiply_fusion
  16.2 0.8 multiply_subtract_fusion.2
  17.0 1.3 dynamic_slice.50
  18.3 1.3 dynamic_slice.53
  21.8 23.3 %all-gather.2 = f32[8,2,1024]{2,1,0:T(2,128)} all-gather(f32[1,2,1024]{2,1,0:T(2,128)S(1)} %maximum_bitcast_fusion), channel_id=2, replica_groups=mesh['sp'=8,'tp'=4] {'sp'}, dimensions={0}, use_global_device_ids=true | all-gather | bytes 73728 | tf_op jit(solution)/shard_map/all_gather | solution.py:15
  45.1 0.9 dynamic-slice_convert_fusion
  46.4 1.0 constant_dynamic-slice_fusion
  47.4 1.9 multiply_bitcast_fusion
  49.3 2.8 %reshape.308 = f32[1024,256]{0,1:T(8,128)} reshape(f32[16,64,16,16]{1,0,3,2:T(8,128)} %get-tuple-element.120) | data formatting | bytes 2097152 | tf_op jit(solution)/shard_map/reshape | solution.py:187
  52.0 1.6 reshape.307
  53.6 1.0 multiply_add_fusion.1
  54.6 1.9 multiply_bitcast_fusion.2
  56.5 2.7 %reshape.306 = f32[256,1024]{1,0:T(8,128)} reshape(f32[16,16,16,64]{3,2,1,0:T(8,128)} %get-tuple-element.126) | data formatting | bytes 2097152 | tf_op jit(solution)/shard_map/reshape | solution.py:152
  61.0 1.8 fusion.1
  62.9 10.9 %all-gather.12.cloned.1.call-done = bf16[3072,256]{1,0:T(8,128)(2,1)} async-done(((bf16[384,256]{1,0:T(8,128)(2,1)}), bf16[3072,256]{1,0:T(8,128)(2,1)}) %all-gather.12.cloned.1.call-update) | async-done | bytes 1572880 | tf_op jit(solution)/shard_map/all_gather | solution.py:108
  73.8 2.7 %fusion.20 = bf16[256,256]{0,1:T(8,128)(2,1)S(1)} fusion(bf16[3072,256]{1,0:T(8,128)(2,1)} %all-gather.12.cloned.1.call-done, bf16[256,3072]{1,0:T(8,128)(2,1)} %all-gather.10.cloned.1.call-done, f32[3072]{0:T(1024)S(1)} %copy-done.38, f32[256]{0:T(256)S(1)} %add_rsqrt_fusion), kind=kOutput, calls=%fused_computation.32 | convolution fusion | flops 405143552 | bytes 3290112 | tf_op jit(solution)/shard_map/dot_general | solution.py:121
  77.2 1.7 slice.477
  78.9 1.4 slice.389
  80.4 1.4 slice.382
  82.5 1.5 slice.474
  84.1 1.5 slice.383
  85.5 1.5 slice.380
  87.0 1.4 add_add_fusion.1
  92.2 0.8 add_add_fusion.5
  98.5 20.1 %all-gather.16.cloned.1.call-done = bf16[3072,256]{1,0:T(8,128)(2,1)} async-done(((bf16[384,256]{1,0:T(8,128)(2,1)}), bf16[3072,256]{1,0:T(8,128)(2,1)}) %all-gather.16.cloned.1.call-update) | async-done | bytes 1572880 | tf_op jit(solution)/shard_map/all_gather | solution.py:109
  118.6 2.2 %fusion.17 = bf16[256,256]{0,1:T(8,128)(2,1)S(1)} fusion(bf16[3072,256]{1,0:T(8,128)(2,1)} %all-gather.16.cloned.1.call-done, bf16[256,3072]{1,0:T(8,128)(2,1)S(1)} %copy-done.8, f32[3072]{0:T(1024)} %param.19, f32[256]{0:T(256)} %copy-done.37), kind=kOutput, calls=%fused_computation.31 | convolution fusion | flops 405143552 | bytes 3290112 | tf_op jit(solution)/shard_map/dot_general | solution.py:122
  121.5 2.4 %collective-permute-start.2 = (bf16[16,256]{0,1:T(8,128)(2,1)}, bf16[16,256]{0,1:T(8,128)(2,1)}, u32[]{:S(2)}, u32[]{:S(2)}) collective-permute-start(bf16[16,256]{0,1:T(8,128)(2,1)} %slice.534), channel_id=1, source_target_pairs={{0,4},{4,8},{8,12},{12,16},{16,20},{20,24},{24,28},{1,5},{5,9},{9,... | collective-permute-start | bytes 24584 | tf_op jit(solution)/shard_map/ppermute | solution.py:29
  127.1 0.9 copy-done.5
  128.2 1.2 add_add_fusion
  129.4 2.7 %pad.126 = f32[256,1024]{1,0:T(8,128)} pad(f32[128,1024]{1,0:T(8,128)S(1)} %pad_maximum_fusion, f32[]{:T(128)} %constant.109.clone.1), padding=0_1_1x0_0_0 | pad | bytes 1572868 | tf_op jit(solution)/shard_map/pad | solution.py:160
  132.3 2.7 %pad.127 = f32[256,1024]{1,0:T(8,128)} pad(f32[128,1024]{1,0:T(8,128)S(1)} %add.699, f32[]{:T(128)} %constant.109.clone.1), padding=1_0_1x0_0_0 | pad | bytes 1572868 | tf_op jit(solution)/shard_map/pad | solution.py:160
  135.0 2.7 %pad.129 = f32[256,1024]{1,0:T(8,128)} pad(f32[128,1024]{1,0:T(8,128)S(1)} %add.702, f32[]{:T(128)} %constant.109.clone.1), padding=1_0_1x0_0_0 | pad | bytes 1572868 | tf_op jit(solution)/shard_map/pad | solution.py:160
  139.3 23.6 %all-gather.3 = f32[8,2,1024]{2,1,0:T(2,128)S(1)} all-gather(f32[1,2,1024]{2,1,0:T(2,128)S(1)} %maximum_bitcast_fusion.1), channel_id=3, replica_groups=mesh['sp'=8,'tp'=4] {'sp'}, dimensions={0}, use_global_device_ids=true | all-gather | bytes 73728 | tf_op jit(solution)/shard_map/all_gather | solution.py:15
  162.9 5.0 %while.12 = (s32[]{:T(128)}, f32[2,1024]{1,0:T(2,128)S(1)}, s32[]{:T(128)}, f32[8,2,1024]{2,1,0:T(2,128)}, f32[8,2,1024]{2,1,0:T(2,128)S(1)}, /*index=5*/s32[]{:T(128)}, s32[]{:T(128)}, s32[]{:T(128)}, s32[]{}) while((s32[]{:T(128)}, f32[2,1024]{1,0:T(2,128)S(1)}, s32[]{:T(128)}, f32[8,2,1024]{2,1,0:T(2,128)}, f32[8,2,1024]{2,1,0:T(2,128)S(1)}, ...), condition=%wide.region_2.3_spmd, body=%wide.region_1.2_spmd.sunk | while | flops 10246 | bytes 49311 | solution.py:23
  163.7 0.8 multiply_subtract_fusion.23
  164.6 0.8 multiply_subtract_fusion.23
  168.0 7.7 %fusion.29 = f32[256,256]{0,1:T(8,128)S(1)} fusion(f32[1024,256]{0,1:T(8,128)} %reshape.307, f32[256,1024]{1,0:T(8,128)} %pad.126, f32[256,1024]{1,0:T(8,128)} %pad.127, f32[1024]{0:T(1024)S(1)} %bitcast.63, f32[1024]{0:T(1024)S(1)} %bitcast.61, f32[1024]{0:T(1024)S(1)} %copy-done.31, f32[1024]{0:T(1024)S(1)} %copy-done.30, f32[256]{0:T(256)S(1)} %copy-done.45), kind=kOutput, calls=%fused_computation.39 | convolution fusion | flops 807665664 | bytes 3425280 | tf_op jit(solution)/shard_map/dot_general | solution.py:190
  175.8 5.2 %constant_dynamic-update-slice_fusion.5 = (bf16[256,2048]{0,1:T(8,128)(2,1)S(1)}, bf16[256,256]{0,1:T(8,128)(2,1)S(1)}) fusion(bf16[256,256]{0,1:T(8,128)(2,1)S(1)} %fusion.20, f32[256]{0:T(256)S(1)} %copy-done.36, f32[256,256]{0,1:T(8,128)S(1)} %fusion.29, f32[1024,256]{0,1:T(8,128)S(1)} %copy-done.10, f32[256,1024]{1,0:T(8,128)S(1)} %pad.128, ...), kind=kOutput, calls=%fused_computation.142 | convolution fusion | flops 808517632 | bytes 3819520 | tf_op jit(solution)/shard_map/dot_general | solution.py:191
  181.1 8.4 %collective-permute-start = (bf16[256,256]{0,1:T(8,128)(2,1)S(1)}, bf16[256,256]{0,1:T(8,128)(2,1)S(1)}, u32[]{:S(2)}, u32[]{:S(2)}) collective-permute-start(bf16[256,256]{0,1:T(8,128)(2,1)S(1)} %get-tuple-element.129), channel_id=1, source_target_pairs={{0,3},{1,0},{2,1},{3,2},{4,7},{5,4},{6,5},{7,6},{8,11},{9,8},{10,9... | collective-permute-start | bytes 393224 | tf_op jit(solution)/shard_map/ppermute | solution.py:102
  189.5 1.2 convolution_select_fusion
  190.8 1.2 convolution_select_fusion.1
  192.1 1.2 convolution_select_fusion.2
  193.3 1.2 fusion.8
  195.2 7.3 %all_gather.38 = bf16[256,1024]{1,0:T(8,128)(2,1)S(1)} all-gather(bf16[256,256]{1,0:T(8,128)(2,1)S(1)} %fusion.16), channel_id=1, replica_groups=mesh['sp'=8,'tp'=4] {'tp'}, dimensions={1}, use_global_device_ids=true | all-gather | bytes 655360 | tf_op jit(solution)/shard_map/all_gather | solution.py:228
  202.5 1.3 collective-permute-start.1
  203.7 2.0 fusion.95
  205.7 4.5 %collective-permute-done.1 = bf16[256,512]{0,1:T(8,128)(2,1)S(1)} collective-permute-done((bf16[256,512]{0,1:T(8,128)(2,1)S(1)}, bf16[256,512]{0,1:T(8,128)(2,1)S(1)}, u32[]{:S(2)}, u32[]{:S(2)}) %collective-permute-start.1) | collective-permute-done | bytes 262176 | tf_op jit(solution)/shard_map/ppermute | solution.py:102
  210.4 2.8 %fusion.6 = bf16[256,768]{1,0:T(8,128)(2,1)} fusion(f32[256,768]{1,0:T(8,128)S(1)} %fusion.95, bf16[1024,768]{1,0:T(8,128)(2,1)} %all-gather.14.cloned.1.call-done, bf16[256,2048]{0,1:T(8,128)(2,1)S(1)} %constant_dynamic-update-slice_fusion, s32[]{:T(128)S(6)} %select_n.94), kind=kOutput, calls=%fused_computation.18 | convolution fusion | flops 403046400 | bytes 3276804 | tf_op jit(solution)/shard_map/dot_general | solution.py:224
  (268 shorter events, 33.0 us)
Async XLA Ops:
  6.5 54.5 %all-gather.10.cloned.1.call-start = ((), (), s32[]{:S(2)}) async-start(), calls=%async_computation | async-start | bytes 1966080 | tf_op jit(solution)/shard_map/all_gather | solution.py:117
  7.3 66.5 %all-gather.12.cloned.1.call-start = ((), (), s32[]{:S(2)}) async-start(), calls=%async_computation.1 | async-start | bytes 1769472 | tf_op jit(solution)/shard_map/all_gather | solution.py:108
  8.0 110.6 %all-gather.16.cloned.1.call-start = ((), (), s32[]{:S(2)}) async-start(), calls=%async_computation.3 | async-start | bytes 1769472 | tf_op jit(solution)/shard_map/all_gather | solution.py:109
  8.7 195.0 %all-gather.18.cloned.1.call-start = ((), (), s32[]{:S(2)}) async-start(), calls=%async_computation.4 | async-start | bytes 1769472 | tf_op jit(solution)/shard_map/all_gather | solution.py:111
  9.3 201.0 %all-gather.14.cloned.1.call-start = ((), (), s32[]{:S(2)}) async-start(), calls=%async_computation.2 | async-start | bytes 1769472 | tf_op jit(solution)/shard_map/all_gather | solution.py:110
  59.8 14.0 %copy-start.38 = (f32[3072]{0:T(1024)S(1)}, f32[3072]{0:T(1024)}, u32[]{:S(2)}) copy-start(f32[3072]{0:T(1024)} %param.19) | copy-start | bytes 36868
  62.8 11.0 %copy-start.37 = (f32[256]{0:T(256)}, f32[256]{0:T(256)S(1)}, u32[]{:S(2)}) copy-start(f32[256]{0:T(256)S(1)} %add_rsqrt_fusion) | copy-start | bytes 3076
  62.8 13.6 %copy-start.2 = (f32[256,1024]{1,0:T(8,128)S(1)}, f32[256,1024]{1,0:T(8,128)}, u32[]{:S(2)}) copy-start(f32[256,1024]{1,0:T(8,128)} %reshape.306) | copy-start | bytes 3145732
  77.2 4.6 %copy-start = (f32[256,1024]{1,0:T(8,128)}, f32[256,1024]{1,0:T(8,128)S(1)}, u32[]{:S(2)}) copy-start(f32[256,1024]{1,0:T(8,128)S(1)} %fusion.94) | copy-start | bytes 3145732
  82.5 4.5 %copy-start.1 = (f32[256,1024]{1,0:T(8,128)}, f32[256,1024]{1,0:T(8,128)S(1)}, u32[]{:S(2)}) copy-start(f32[256,1024]{1,0:T(8,128)S(1)} %fusion.93) | copy-start | bytes 3145732
  82.5 4.5 %copy-start.3 = (f32[128,1024]{1,0:T(8,128)S(1)}, f32[128,1024]{1,0:T(8,128)}, u32[]{:S(2)}) copy-start(f32[128,1024]{1,0:T(8,128)} %slice.389) | copy-start | bytes 1572868
  82.5 4.5 %copy-start.4 = (f32[128,1024]{1,0:T(8,128)S(1)}, f32[128,1024]{1,0:T(8,128)}, u32[]{:S(2)}) copy-start(f32[128,1024]{1,0:T(8,128)} %slice.382) | copy-start | bytes 1572868
  89.0 1.6 copy-start.11
  89.0 1.6 copy-start.13
  92.2 26.4 %copy-start.8 = (bf16[256,3072]{1,0:T(8,128)(2,1)S(1)}, bf16[256,3072]{1,0:T(8,128)(2,1)}, u32[]{:S(2)}) copy-start(bf16[256,3072]{1,0:T(8,128)(2,1)} %all-gather.10.cloned.1.call-done) | copy-start | bytes 4718596
  98.5 25.8 %copy-start.19 = (f32[1024]{0:T(1024)S(1)}, f32[1024]{0:T(1024)}, u32[]{:S(2)}) copy-start(f32[1024]{0:T(1024)} %get-tuple-element.66) | copy-start | bytes 12292
  98.5 25.8 %copy-start.20 = (f32[1024]{0:T(1024)S(1)}, f32[1024]{0:T(1024)}, u32[]{:S(2)}) copy-start(f32[1024]{0:T(1024)} %get-tuple-element.67) | copy-start | bytes 12292
  120.8 3.9 %copy-start.21 = (bf16[256,256]{0,1:T(8,128)(2,1)}, bf16[256,256]{0,1:T(8,128)(2,1)S(1)}, u32[]{:S(2)}) copy-start(bf16[256,256]{0,1:T(8,128)(2,1)S(1)} %fusion.17) | copy-start | bytes 393220
  120.8 3.8 %copy-start.17 = (f32[1024]{0:T(1024)S(1)}, f32[1024]{0:T(1024)}, u32[]{:S(2)}) copy-start(f32[1024]{0:T(1024)} %get-tuple-element.68) | copy-start | bytes 12292
  120.8 3.8 %copy-start.18 = (f32[1024]{0:T(1024)S(1)}, f32[1024]{0:T(1024)}, u32[]{:S(2)}) copy-start(f32[1024]{0:T(1024)} %get-tuple-element.69) | copy-start | bytes 12292
  120.8 3.8 %copy-start.28 = (f32[1,1024]{1,0:T(1,128)S(1)}, f32[1,1024]{1,0:T(1,128)}, u32[]{:S(2)}) copy-start(f32[1,1024]{1,0:T(1,128)} %slice.485) | copy-start | bytes 12292
  120.8 3.8 %copy-start.27 = (f32[1,1024]{1,0:T(1,128)S(1)}, f32[1,1024]{1,0:T(1,128)}, u32[]{:S(2)}) copy-start(f32[1,1024]{1,0:T(1,128)} %slice.516) | copy-start | bytes 12292
  121.5 68.0 %collective-permute-start.2 = (bf16[16,256]{0,1:T(8,128)(2,1)}, bf16[16,256]{0,1:T(8,128)(2,1)}, u32[]{:S(2)}, u32[]{:S(2)}) collective-permute-start(bf16[16,256]{0,1:T(8,128)(2,1)} %slice.534), channel_id=1, source_target_pairs={{0,4},{4,8},{8,12},{12,16},{16,20},{20,24},{24,28},{1,5},{5,9},{9,... | collective-permute-start | bytes 24584 | tf_op jit(solution)/shard_map/ppermute | solution.py:29
  127.0 1.0 copy-start.5
  127.0 1.2 copy-start.6
  128.2 1.2 slice-start.1
  129.3 2.8 %slice-start = ((f32[256,1024]{1,0:T(8,128)}), f32[1,1024]{1,0:T(1,128)S(1)}, s32[]{:S(2)}) async-start(f32[256,1024]{1,0:T(8,128)} %copy-done), calls=%async_computation.5 | async-start | bytes 8192 | tf_op jit(solution)/shard_map/slice | solution.py:160
  129.3 2.8 %copy-start.7 = (f32[127,1024]{1,0:T(8,128)S(1)}, f32[127,1024]{1,0:T(8,128)}, u32[]{:S(2)}) copy-start(f32[127,1024]{1,0:T(8,128)} %get-tuple-element.79) | copy-start | bytes 1560580
  132.3 35.6 %copy-start.30 = (f32[1024]{0:T(1024)S(1)}, f32[1024]{0:T(1024)}, u32[]{:S(2)}) copy-start(f32[1024]{0:T(1024)} %mul.1010) | copy-start | bytes 12292
  132.3 35.6 %copy-start.31 = (f32[1024]{0:T(1024)S(1)}, f32[1024]{0:T(1024)}, u32[]{:S(2)}) copy-start(f32[1024]{0:T(1024)} %mul.1013) | copy-start | bytes 12292
  132.3 35.6 %copy-start.45 = (f32[256]{0:T(256)S(1)}, f32[256]{0:T(256)}, u32[]{:S(2)}) copy-start(f32[256]{0:T(256)} %iota_add_fusion.4) | copy-start | bytes 3076
  168.0 7.8 %copy-start.9 = (f32[256,1024]{1,0:T(8,128)S(1)}, f32[256,1024]{1,0:T(8,128)}, u32[]{:S(2)}) copy-start(f32[256,1024]{1,0:T(8,128)} %pad.129) | copy-start | bytes 3145732
  168.0 7.8 %copy-start.10 = (f32[1024,256]{0,1:T(8,128)S(1)}, f32[1024,256]{0,1:T(8,128)}, u32[]{:S(2)}) copy-start(f32[1024,256]{0,1:T(8,128)} %reshape.308) | copy-start | bytes 3145732
  168.0 7.8 %copy-start.36 = (f32[256]{0:T(256)S(1)}, f32[256]{0:T(256)}, u32[]{:S(2)}) copy-start(f32[256]{0:T(256)} %dynamic_slice.50) | copy-start | bytes 3076
  175.8 13.8 %copy-start.22 = (bf16[256,256]{0,1:T(8,128)(2,1)S(1)}, bf16[256,256]{0,1:T(8,128)(2,1)}, u32[]{:S(2)}) copy-start(bf16[256,256]{0,1:T(8,128)(2,1)} %copy-done.21) | copy-start | bytes 393220
  175.8 13.7 %copy-start.34 = (s32[256]{0:T(256)S(1)}, s32[256]{0:T(256)}, u32[]{:S(2)}) copy-start(s32[256]{0:T(256)} %get-tuple-element.141) | copy-start | bytes 3076
  175.8 13.7 %copy-start.35 = (s32[256]{0:T(256)S(1)}, s32[256]{0:T(256)}, u32[]{:S(2)}) copy-start(s32[256]{0:T(256)} %get-tuple-element.140) | copy-start | bytes 3076
  175.8 13.7 %copy-start.42 = (pred[256]{0:T(512)(128)(4,1)S(1)}, pred[256]{0:T(512)(128)(4,1)}, u32[]{:S(2)}) copy-start(pred[256]{0:T(512)(128)(4,1)} %get-tuple-element.130) | copy-start | bytes 772
  175.8 15.0 %copy-start.40 = (pred[256]{0:T(512)(128)(4,1)S(1)}, pred[256]{0:T(512)(128)(4,1)}, u32[]{:S(2)}) copy-start(pred[256]{0:T(512)(128)(4,1)} %get-tuple-element.133) | copy-start | bytes 772
  175.8 15.0 %copy-start.44 = (s32[256]{0:T(256)S(1)}, s32[256]{0:T(256)}, u32[]{:S(2)}) copy-start(s32[256]{0:T(256)} %iota_add_fusion.1) | copy-start | bytes 3076
  181.0 11.0 %copy-start.41 = (pred[256]{0:T(512)(128)(4,1)S(1)}, pred[256]{0:T(512)(128)(4,1)}, u32[]{:S(2)}) copy-start(pred[256]{0:T(512)(128)(4,1)} %get-tuple-element.131) | copy-start | bytes 772
  181.1 11.0 %copy-start.43 = (s32[256]{0:T(256)S(1)}, s32[256]{0:T(256)}, u32[]{:S(2)}) copy-start(s32[256]{0:T(256)} %iota_add_fusion.2) | copy-start | bytes 3076
  181.1 12.3 %copy-start.32 = (s32[256]{0:T(256)S(1)}, s32[256]{0:T(256)}, u32[]{:S(2)}) copy-start(s32[256]{0:T(256)} %get-tuple-element.142) | copy-start | bytes 3076
  181.1 12.3 %copy-start.33 = (s32[256]{0:T(256)S(1)}, s32[256]{0:T(256)}, u32[]{:S(2)}) copy-start(s32[256]{0:T(256)} %get-tuple-element.143) | copy-start | bytes 3076
  181.1 12.3 %copy-start.39 = (pred[256]{0:T(512)(128)(4,1)S(1)}, pred[256]{0:T(512)(128)(4,1)}, u32[]{:S(2)}) copy-start(pred[256]{0:T(512)(128)(4,1)} %get-tuple-element.132) | copy-start | bytes 772
  181.1 21.4 %collective-permute-start = (bf16[256,256]{0,1:T(8,128)(2,1)S(1)}, bf16[256,256]{0,1:T(8,128)(2,1)S(1)}, u32[]{:S(2)}, u32[]{:S(2)}) collective-permute-start(bf16[256,256]{0,1:T(8,128)(2,1)S(1)} %get-tuple-element.129), channel_id=1, source_target_pairs={{0,3},{1,0},{2,1},{3,2},{4,7},{5,4},{6,5},{7,6},{8,11},{9,8},{10,9... | collective-permute-start | bytes 393224 | tf_op jit(solution)/shard_map/ppermute | solution.py:102
  192.0 2.5 %copy-start.29 = (f32[256]{0:T(256)S(1)}, f32[256]{0:T(256)}, u32[]{:S(2)}) copy-start(f32[256]{0:T(256)} %dynamic_slice.53) | copy-start | bytes 3076
  202.5 7.8 %collective-permute-start.1 = (bf16[256,512]{0,1:T(8,128)(2,1)S(1)}, bf16[256,512]{0,1:T(8,128)(2,1)S(1)}, u32[]{:S(2)}, u32[]{:S(2)}) collective-permute-start(bf16[256,512]{0,1:T(8,128)(2,1)S(1)} %pad_maximum_fusion.4), channel_id=1, source_target_pairs={{0,2},{1,3},{2,0},{3,1},{4,6},{5,7},{6,4},{7,5},{8,10},{9,11},{10,... | collective-permute-start | bytes 786440 | tf_op jit(solution)/shard_map/ppermute | solution.py:102
  (8 other events, 5.4 us)
Sparse Core Ops, SparseCore 0:
  8.9 20.9 all-gather.9
  32.1 41.6 all-gather.11
  76.0 42.5 all-gather.15
  120.6 43.2 all-gather.17
  165.9 42.4 all-gather.13
